TPU v7x, 32 devices: a whole 2x2x4 slice. The times are simulated.
32 devices in a mesh: kv: 16 (over z, y, core), tp: 2 (over x).
Axes of the slice: x: 2, y: 2, z: 4, core: 2. Of those that a mesh axis runs over, the one named last changes fastest.
Arguments:
- hidden_in: bfloat16 [32, 3072], replicated, may hold values from -60 to 60
- in_gain: bfloat16 [3072], replicated, may hold values from 0.099609375 to 1.8984375
- query_weight: bfloat16 [3072, 1536], P(None, 'tp'), may hold values from -0.109375 to 0.109375
- key_weight: bfloat16 [3072, 256], replicated, may hold values from -0.109375 to 0.109375
- value_weight: bfloat16 [3072, 256], replicated, may hold values from -0.109375 to 0.109375
- key_cache: bfloat16 [32, 2, 1024, 128], P(None, None, 'kv'), may hold values from -200 to 200
- value_cache: bfloat16 [32, 2, 1024, 128], P(None, None, 'kv'), may hold values from -6 to 6
- lengths: int32 [32], replicated, may hold values from 256 to 1023
- mix_lambda: float32 [12], P('tp'), may hold values from 0.3 to 0.8
- head_gain: bfloat16 [12, 128], P('tp'), may hold values from 0.099609375 to 1.8984375
- out_weight: bfloat16 [1536, 3072], P('tp', 'kv'), may hold values from -0.15625 to 0.15625
Outputs:
- mixed: bfloat16 [32, 3072], P(None, 'kv')
- new_keys: bfloat16 [32, 2, 128], replicated
- new_values: bfloat16 [32, 2, 128], replicated
All inputs are finite; a program needn't handle non-finite values.
Results may differ from a plain program's by a relative error of at most 0.013.
The roundings to bfloat16 on the way count: a program that leaves them out, or rounds other values in their place, can miss the bound.
Values may be sent and summed in bfloat16 or wider, within the bound.
A program may use at most 64 MiB of HBM per device.

v0:
```python
import functools
import math

import jax
import jax.numpy as jnp
import numpy as np
from jax import lax
from jax.experimental import pallas as pl
from jax.experimental.pallas import tpu as pltpu
from jax.sharding import PartitionSpec as P

HEADS = 12
KV_HEADS = 2


EPS = 1e-06
THETA = 500000.0
NEG = -1e30


def joined(value, axis, join):
    pieces = jax.tree.map(lambda part: lax.all_gather(part, axis), value)
    head = jax.tree.map(lambda part: part[0], pieces)
    tail = jax.tree.map(lambda part: part[1:], pieces)
    subtotal, _ = lax.scan(lambda subtotal, section: (join(subtotal, section), None), head, tail)
    return subtotal


def rotate(vectors, position):
    half_dim = vectors.shape[-1] // 2
    frequency = THETA ** (-jnp.arange(half_dim, dtype=jnp.float32) * 2.0 / vectors.shape[-1])
    angles = position[:, None, None, None] * frequency
    cosine = jnp.cos(angles)
    sine_part = jnp.sin(angles)
    lower_half = vectors[..., :half_dim]
    upper_half = vectors[..., half_dim:]
    return jnp.concatenate(
        [
            lower_half * cosine - upper_half * sine_part,
            upper_half * cosine + lower_half * sine_part,
        ],
        axis=-1,
    )


def merge_parts(earlier, later):
    max_early, sum_early, values_early = earlier
    max_late, sum_late, values_late = later
    joint = jnp.maximum(max_early, max_late)
    early_factor = jnp.exp(max_early - joint)
    late_factor = jnp.exp(max_late - joint)
    return (
        joint,
        sum_early * early_factor + sum_late * late_factor,
        values_early * early_factor[..., None] + values_late * late_factor[..., None],
    )


def per_device(
    hidden_in,
    in_gain,
    query_weight,
    key_weight,
    value_weight,
    key_cache,
    value_cache,
    lengths,
    mix_lambda,
    head_gain,
    out_weight,
):
    seq_count = hidden_in.shape[0]
    local_heads = mix_lambda.shape[0]
    head_dim = query_weight.shape[1] // (2 * local_heads)
    kv_count = key_cache.shape[1]
    span_len = key_cache.shape[2]
    value_dim = value_cache.shape[3]
    inputs = hidden_in.astype(jnp.float32)
    inverse = lax.rsqrt(jnp.mean(inputs * inputs, axis=-1, keepdims=True) + EPS)
    scaled = (inputs * in_gain.astype(jnp.float32)).astype(jnp.bfloat16)
    position = lengths.astype(jnp.float32)
    query_part = jnp.dot(scaled, query_weight, preferred_element_type=jnp.float32)
    key_part = jnp.dot(scaled, key_weight, preferred_element_type=jnp.float32)
    value_part = jnp.dot(scaled, value_weight, preferred_element_type=jnp.float32)
    queries = rotate(
        (query_part * inverse).reshape(seq_count, local_heads, 2, head_dim), position
    ).astype(jnp.bfloat16)
    new_keys = rotate(
        (key_part * inverse).reshape(seq_count, kv_count, 2, head_dim), position
    ).astype(jnp.bfloat16)
    new_values = (value_part * inverse).astype(jnp.bfloat16).reshape(seq_count, kv_count, value_dim)
    group_size = HEADS // KV_HEADS
    kv_index = lax.axis_index("tp") * local_heads // group_size
    own_keys = lax.dynamic_slice_in_dim(key_cache, kv_index, 1, 1)[:, 0].reshape(
        seq_count, span_len, 2, head_dim
    )
    own_values = lax.dynamic_slice_in_dim(value_cache, kv_index, 1, 1)[:, 0]
    scale_root = math.sqrt(head_dim)
    scores = (
        jnp.einsum("bmcd,bpcd->bmcp", queries, own_keys, preferred_element_type=jnp.float32)
        / scale_root
    )
    places = lax.axis_index("kv") * span_len + jnp.arange(span_len, dtype=jnp.int32)
    visible = (places[None, :] < lengths[:, None])[:, None, None, :]
    scores = jnp.where(visible, scores, NEG)
    local_max = jnp.max(scores, axis=-1)
    weights = jnp.where(visible, jnp.exp(scores - local_max[..., None]), 0.0)
    local_sum = jnp.sum(weights, axis=-1)
    local_values = jnp.einsum(
        "bmcp,bpe->bmce",
        weights.astype(jnp.bfloat16),
        own_values,
        preferred_element_type=jnp.float32,
    )
    running_max, running_sum, weighted = joined(
        (local_max, local_sum, local_values), "kv", merge_parts
    )
    own_key = lax.dynamic_slice_in_dim(new_keys, kv_index, 1, 1)[:, 0].astype(jnp.float32)
    own_value = lax.dynamic_slice_in_dim(new_values, kv_index, 1, 1)[:, 0].astype(jnp.float32)
    own_scores = jnp.einsum("bmcd,bcd->bmc", queries.astype(jnp.float32), own_key) / scale_root
    joint = jnp.maximum(running_max, own_scores)
    past_factor = jnp.exp(running_max - joint)
    own_weight = jnp.exp(own_scores - joint)
    running_sum = running_sum * past_factor + own_weight
    weighted = (
        weighted * past_factor[..., None] + own_weight[..., None] * own_value[:, None, None, :]
    )
    outputs = weighted / running_sum[..., None]
    lambda_rows = mix_lambda[None, :, None]
    head_out = outputs[:, :, 0, :] - lambda_rows * outputs[:, :, 1, :]
    normed = (
        head_out
        * lax.rsqrt(jnp.mean(head_out * head_out, axis=-1, keepdims=True) + EPS)
        * head_gain.astype(jnp.float32)
    ).astype(jnp.bfloat16)
    partial_out = jnp.dot(
        normed.reshape(seq_count, local_heads * value_dim),
        out_weight,
        preferred_element_type=jnp.float32,
    ).astype(jnp.bfloat16)
    partial_out = lax.optimization_barrier(partial_out).astype(jnp.float32)
    mixed = lax.psum(partial_out.astype(jnp.bfloat16), "tp")
    return (mixed, new_keys.reshape(seq_count, kv_count, 2 * head_dim), new_values)


MESH = pl.DeviceIdType.MESH
CHUNKS = 4


def fused_kernel(
    dims,
    hidden_h,
    gain_h,
    lens_h,
    lam_h,
    head_gain_h,
    freq_h,
    expand_h,
    owner_seq_h,
    lane_pos_h,
    collect_h,
    query_w,
    key_w,
    value_w,
    key_c,
    value_c,
    out_w,
    mixed,
    new_keys,
    new_values,
    hidden,
    gain,
    lens,
    lam,
    head_gain,
    freq,
    expand,
    owner_seq,
    lane_pos,
    collect,
    qw_v,
    kw_v,
    vw_v,
    kc_v,
    vc_v,
    ow_v,
    scaled_v,
    q_v,
    qrows,
    limits,
    own_kv,
    vsend,
    vrecv,
    srecv,
    gain_rows,
    pad_v,
    nbuf,
    pbuf,
    in_sem,
    small_sem,
    vs_sem,
    vr_sem,
    ns_sem,
    nr_sem,
    ps_sem,
    pr_sem,
):
    n, tp, seqs, lh, kvc, span, head_dim, vd, group = dims
    spo = seqs // n
    ro = 2 * spo * lh
    half = spo * lh
    npair = n // 2
    width = 2 * head_dim
    me = lax.axis_index("kv")
    tpi = lax.axis_index("tp")
    par = lax.rem(me, 2)
    pair = lax.div(me, 2)
    kvh = lax.div(tpi * lh, group)
    d = hidden.shape[1]
    ck = d // CHUNKS

    small = []
    for i, (src, dst) in enumerate(
        (
            (hidden_h, hidden),
            (gain_h, gain),
            (lens_h, lens),
            (freq_h, freq),
            (owner_seq_h, owner_seq),
            (head_gain_h, head_gain),
            (lam_h, lam),
            (expand_h, expand),
            (lane_pos_h, lane_pos),
            (collect_h, collect),
        )
    ):
        cp = pltpu.make_async_copy(src, dst, small_sem.at[i])
        cp.start()
        small.append(cp)
    q_copies = []
    for i in range(CHUNKS):
        rows = pl.ds(i * ck, ck)
        cp = pltpu.make_async_copy(query_w.at[rows], qw_v.at[rows], in_sem.at[i])
        cp.start()
        q_copies.append(cp)
    kc_cp = pltpu.make_async_copy(key_c.at[:, kvh], kc_v, in_sem.at[CHUNKS])
    vc_cp = pltpu.make_async_copy(value_c.at[:, kvh], vc_v, in_sem.at[CHUNKS + 1])
    kw_cp = pltpu.make_async_copy(key_w, kw_v, in_sem.at[CHUNKS + 2])
    vw_cp = pltpu.make_async_copy(value_w, vw_v, in_sem.at[CHUNKS + 3])
    ow_cp = pltpu.make_async_copy(out_w, ow_v, in_sem.at[CHUNKS + 4])
    kc_cp.start()
    vc_cp.start()

    barrier = pltpu.get_barrier_semaphore()
    for k in range(1, n):
        pl.semaphore_signal(
            barrier, inc=1, device_id=(lax.rem(me + k, n), tpi), device_id_type=MESH
        )
    for k in range(1, tp):
        pl.semaphore_signal(
            barrier, inc=1, device_id=(me, lax.rem(tpi + k, tp)), device_id_type=MESH
        )

    for cp in small[:6]:
        cp.wait()
    inputs = hidden[...].astype(jnp.float32)
    inverse = lax.rsqrt(jnp.mean(inputs * inputs, axis=-1, keepdims=True) + EPS)
    scaled_v[...] = (inputs * gain[...].astype(jnp.float32)[None, :]).astype(jnp.bfloat16)
    lens_f = lens[...].astype(jnp.float32)
    rr = lax.broadcasted_iota(jnp.int32, (seqs, seqs), 0)
    cc = lax.broadcasted_iota(jnp.int32, (seqs, seqs), 1)
    lens_col = jnp.sum(jnp.where(rr == cc, lens_f, 0.0), axis=1, keepdims=True)
    angles = lens_col * freq[...]
    lane = lax.broadcasted_iota(jnp.int32, (seqs, width), 1)
    low = lax.rem(lane, head_dim) < head_dim // 2
    first = lane < head_dim
    cosine = jnp.cos(angles)
    sine = jnp.sin(angles)
    signed = jnp.where(low, -sine, sine)

    def turn(x):
        other = jnp.where(
            low,
            pltpu.roll(x, width - head_dim // 2, 1),
            pltpu.roll(x, head_dim // 2, 1),
        )
        return x * cosine + other * signed

    rel = jnp.clip(lens_col - (me * span).astype(jnp.float32), 0.0, float(span))
    rel = jnp.broadcast_to(rel, (seqs, width)).astype(jnp.bfloat16)
    limits[...] = jnp.dot(
        owner_seq[...], rel, preferred_element_type=jnp.float32
    ).reshape(n, ro, width)
    for b in range(spo):
        gain_rows[pl.ds(b * lh, lh), :] = head_gain[...].astype(jnp.float32)
    pad_v[...] = jnp.zeros_like(pad_v)

    acc = jnp.zeros((seqs, lh * width), jnp.float32)
    for i in range(CHUNKS):
        q_copies[i].wait()
        if i == CHUNKS - 1:
            kw_cp.start()
            vw_cp.start()
            ow_cp.start()
        acc = acc + jnp.dot(
            scaled_v[:, i * ck : (i + 1) * ck],
            qw_v[i * ck : (i + 1) * ck, :],
            preferred_element_type=jnp.float32,
        )
    for m in range(lh):
        t = turn(acc[:, m * width : (m + 1) * width] * inverse)
        q_v[pl.ds(m * seqs, seqs), :] = jnp.where(first, t, 0.0).astype(jnp.bfloat16)
        q_v[pl.ds((lh + m) * seqs, seqs), :] = jnp.where(first, 0.0, t).astype(jnp.bfloat16)
    for cp in small[6:]:
        cp.wait()
    qrows[...] = jnp.dot(
        expand[...], q_v[...], preferred_element_type=jnp.float32
    ).reshape(n, ro, width)

    scale = 1.0 / math.sqrt(head_dim)
    rid = lax.broadcasted_iota(jnp.int32, (ro, vd), 0)
    lid = lax.broadcasted_iota(jnp.int32, (ro, vd), 1)
    tail_row = lax.broadcasted_iota(jnp.int32, (8, vd), 0)
    at_max = lid == rid
    at_sum = lid == rid + vd // 2
    kc_cp.wait()
    vc_cp.wait()
    gs = 2 * spo
    order = sorted(range(1, npair), key=lambda k: -min(k, npair - k)) + [0]
    sends = []

    def send(k):
        gi = lax.rem(pair + k, npair)
        for j in range(2):
            if k == 0 and j == 0:
                continue
            t = 2 * gi + par + j * (1 - 2 * par)
            slot = 2 * k + j
            cp = pltpu.make_async_remote_copy(
                src_ref=vsend.at[t],
                dst_ref=vrecv.at[slot],
                send_sem=vs_sem.at[slot],
                recv_sem=vr_sem.at[slot],
                device_id=(t, tpi),
                device_id_type=MESH,
            )
            cp.start()
            sends.append(cp)

    def place(k):
        return lax.rem(pair + k, npair)

    batch = max(1, npair // 2)
    for start in range(0, npair, batch):
        ks = order[start : start + batch]
        scores = []
        for k in ks:
            gi = place(k)
            q = qrows[pl.ds(2 * gi, 2)].reshape(2 * ro, width).astype(jnp.bfloat16)
            keys = kc_v[pl.ds(gi * gs, gs)].reshape(gs * span, width)
            scores.append(
                lax.dot_general(
                    q, keys, (((1,), (1,)), ((), ())), preferred_element_type=jnp.float32
                )
            )
        soft = []
        for k, s in zip(ks, scores):
            lim = limits[pl.ds(2 * place(k), 2)].reshape(2 * ro, width)
            visible = lane_pos[...] < lim[:, :1]
            s = jnp.where(visible, s * scale, NEG)
            mx = jnp.max(s, axis=1, keepdims=True)
            w = jnp.where(visible, jnp.exp(s - mx), 0.0)
            soft.append((mx, jnp.sum(w, axis=1, keepdims=True), w.astype(jnp.bfloat16)))
        values = []
        for k, (_, _, w) in zip(ks, soft):
            vals = vc_v[pl.ds(place(k) * gs, gs)].reshape(gs * span, vd)
            values.append(jnp.dot(w, vals, preferred_element_type=jnp.float32))
        for k, (mx, sm, _), o in zip(ks, soft, values):
            gi = place(k)
            for j in range(2):
                rows = slice(j * ro, (j + 1) * ro)
                stat = jnp.where(at_max, mx[rows], jnp.where(at_sum, sm[rows], 0.0))
                stat = jnp.sum(stat, axis=0, keepdims=True)
                high = stat.astype(jnp.bfloat16).astype(jnp.float32)
                middle = (stat - high).astype(jnp.bfloat16).astype(jnp.float32)
                lowest = stat - high - middle
                tail = jnp.where(
                    tail_row == 0,
                    high,
                    jnp.where(tail_row == 1, middle, jnp.where(tail_row == 2, lowest, 0.0)),
                )
                both = jnp.concatenate([o[rows], tail], axis=0)
                vsend[2 * gi + j] = both.astype(jnp.bfloat16)
        if start == 0:
            pl.semaphore_wait(barrier, n - 1 + tp - 1)
        for k in ks:
            send(k)

    kw_cp.wait()
    kp = jnp.dot(scaled_v[...], kw_v[...], preferred_element_type=jnp.float32) * inverse
    vw_cp.wait()
    vp = jnp.dot(scaled_v[...], vw_v[...], preferred_element_type=jnp.float32) * inverse
    for g in range(kvc):
        nk = turn(kp[:, g * width : (g + 1) * width]).astype(jnp.bfloat16)
        nv = vp[:, g * vd : (g + 1) * vd].astype(jnp.bfloat16)
        new_keys[:, g * width : (g + 1) * width] = nk
        new_values[:, g * vd : (g + 1) * vd] = nv
        own_kv[0, g] = nk
        own_kv[1, g] = nv
    sr = lax.broadcasted_iota(jnp.int32, (ro, seqs), 0)
    sc = lax.broadcasted_iota(jnp.int32, (ro, seqs), 1)
    pick = (sc == me * spo + lax.div(lax.rem(sr, half), lh)).astype(jnp.float32)
    pick = pick.astype(jnp.bfloat16)
    kx = jnp.dot(pick, own_kv[0, kvh], preferred_element_type=jnp.float32)
    vx = jnp.dot(pick, own_kv[1, kvh], preferred_element_type=jnp.float32)
    own = jnp.sum(qrows[me] * kx, axis=1, keepdims=True) * scale
    lam_row = lax.broadcasted_iota(jnp.int32, (half, lh), 0)
    lam_col = lax.broadcasted_iota(jnp.int32, (half, lh), 1)
    mix = jnp.sum(
        jnp.where(lax.rem(lam_row, lh) == lam_col, lam[...], 0.0), axis=1, keepdims=True
    )

    vrecv[0] = vsend[me]
    for cp in sends:
        cp.wait()
    for s in range(n):
        tail = vrecv[s].astype(jnp.float32)[ro:]
        srecv[s : s + 1, :] = tail[0:1] + tail[1:2] + tail[2:3]
    stats = jnp.transpose(srecv[...])
    maxima = stats[:ro]
    sums = stats[vd // 2 : vd // 2 + ro]
    top = jnp.maximum(jnp.max(maxima, axis=1, keepdims=True), own)
    factor = jnp.exp(maxima - top)
    own_w = jnp.exp(own - top)
    total = jnp.sum(factor * sums, axis=1, keepdims=True) + own_w
    weighted = own_w * vx
    for s in range(n):
        weighted = weighted + factor[:, s : s + 1] * vrecv[s].astype(jnp.float32)[:ro]
    outputs = weighted / total
    head_out = outputs[:half] - mix * outputs[half:]
    norm = lax.rsqrt(jnp.mean(head_out * head_out, axis=-1, keepdims=True) + EPS)
    pad_v[pl.ds(0, half), :] = head_out * norm * gain_rows[...]
    nbuf[me] = pad_v[...].astype(jnp.bfloat16)
    sends = []
    for k in range(1, n):
        cp = pltpu.make_async_remote_copy(
            src_ref=nbuf.at[me],
            dst_ref=nbuf.at[me],
            send_sem=ns_sem.at[k],
            recv_sem=nr_sem.at[k],
            device_id=(lax.rem(me + k, n), tpi),
            device_id_type=MESH,
        )
        cp.start()
        sends.append(cp)
    ow_cp.wait()
    for cp in sends:
        cp.wait()
    rows_in = nbuf[...].reshape(nbuf.shape[0] * nbuf.shape[1], vd)
    normed = jnp.dot(collect[...], rows_in, preferred_element_type=jnp.float32).astype(
        jnp.bfloat16
    )
    part = jnp.zeros((seqs, ow_v.shape[0]), jnp.float32)
    for m in range(lh):
        part = part + lax.dot_general(
            normed[m * seqs : (m + 1) * seqs],
            ow_v[:, m * vd : (m + 1) * vd],
            (((1,), (1,)), ((), ())),
            preferred_element_type=jnp.float32,
        )
    pbuf[0] = part.astype(jnp.bfloat16)
    sends = []
    for k in range(1, tp):
        cp = pltpu.make_async_remote_copy(
            src_ref=pbuf.at[0],
            dst_ref=pbuf.at[k],
            send_sem=ps_sem.at[k],
            recv_sem=pr_sem.at[k],
            device_id=(me, lax.rem(tpi + k, tp)),
            device_id_type=MESH,
        )
        cp.start()
        sends.append(cp)
    for cp in sends:
        cp.wait()
    summed = pbuf[0].astype(jnp.float32)
    for k in range(1, tp):
        summed = summed + pbuf[k].astype(jnp.float32)
    mixed[...] = summed.astype(jnp.bfloat16)


def tables(n, seqs, lh, span, head_dim, pad):
    spo = seqs // n
    half = spo * lh
    ro = 2 * half
    row = np.arange(n * ro)
    owner, rem = row // ro, row % ro
    pair_map, b, m = rem // half, owner * spo + (rem % half) // lh, rem % lh
    expand = np.zeros((n * ro, 2 * lh * seqs), np.float32)
    expand[row, (pair_map * lh + m) * seqs + b] = 1.0
    owner_seq = np.zeros((n * ro, seqs), np.float32)
    owner_seq[row, b] = 1.0
    lanes = np.arange(2 * spo * span)
    lane_pos = np.where(
        (b[: 2 * ro])[:, None] == (lanes // span)[None, :], lanes % span, 1 << 20
    ).astype(np.float32)
    collect = np.zeros((lh * seqs, n * pad), np.float32)
    for h in range(lh):
        for s in range(seqs):
            collect[h * seqs + s, (s // spo) * pad + (s % spo) * lh + h] = 1.0
    half_dim = head_dim // 2
    freq = THETA ** (-np.arange(half_dim) * 2.0 / head_dim)
    freq = np.tile(freq, 4)[None, :].astype(np.float32)
    bf = lambda a: jnp.asarray(a, jnp.bfloat16)
    return jnp.asarray(freq), bf(expand), bf(owner_seq), jnp.asarray(lane_pos), bf(collect)


def fused_device(mesh_shape, *args):
    (
        hidden_in,
        in_gain,
        query_weight,
        key_weight,
        value_weight,
        key_cache,
        value_cache,
        lengths,
        mix_lambda,
        head_gain,
        out_weight,
    ) = args
    n, tp = mesh_shape
    seqs, d = hidden_in.shape
    lh = mix_lambda.shape[0]
    head_dim = query_weight.shape[1] // (2 * lh)
    width = 2 * head_dim
    _, kvc, span, vd = value_cache.shape
    spo = seqs // n
    ro = 2 * spo * lh
    pad = -(-(ro // 2) // 16) * 16
    dims = (n, tp, seqs, lh, kvc, span, head_dim, vd, HEADS // KV_HEADS)
    bf, f32 = jnp.bfloat16, jnp.float32
    vmem = pl.BlockSpec(memory_space=pltpu.VMEM)
    hbm = pl.BlockSpec(memory_space=pltpu.HBM)
    dma = pltpu.SemaphoreType.DMA
    consts = tables(n, seqs, lh, span, head_dim, pad)
    smalls = (
        hidden_in,
        in_gain,
        lengths.reshape(1, seqs),
        mix_lambda.reshape(1, lh),
        head_gain,
        *consts,
    )
    out_weight = jnp.transpose(out_weight)
    features = out_weight.shape[0]
    mixed, nk, nv = pl.pallas_call(
        functools.partial(fused_kernel, dims),
        name="fused",
        out_shape=(
            jax.ShapeDtypeStruct((seqs, features), bf),
            jax.ShapeDtypeStruct((seqs, kvc * width), bf),
            jax.ShapeDtypeStruct((seqs, kvc * vd), bf),
        ),
        in_specs=[hbm] * 16,
        out_specs=(vmem, vmem, vmem),
        scratch_shapes=[pltpu.VMEM(a.shape, a.dtype) for a in smalls]
        + [
            pltpu.VMEM(query_weight.shape, bf),
            pltpu.VMEM(key_weight.shape, bf),
            pltpu.VMEM(value_weight.shape, bf),
            pltpu.VMEM((seqs, span, width), bf),
            pltpu.VMEM((seqs, span, vd), bf),
            pltpu.VMEM(out_weight.shape, bf),
            pltpu.VMEM((seqs, d), bf),
            pltpu.VMEM((2 * lh * seqs, width), bf),
            pltpu.VMEM((n, ro, width), f32),
            pltpu.VMEM((n, ro, width), f32),
            pltpu.VMEM((2, kvc, seqs, width), bf),
            pltpu.VMEM((n, ro + 8, vd), bf),
            pltpu.VMEM((n, ro + 8, vd), bf),
            pltpu.VMEM((n, vd), f32),
            pltpu.VMEM((ro // 2, vd), f32),
            pltpu.VMEM((pad, vd), f32),
            pltpu.VMEM((n, pad, vd), bf),
            pltpu.VMEM((tp, seqs, features), bf),
            dma((CHUNKS + 5,)),
            dma((10,)),
        ]
        + [dma((n,))] * 4
        + [dma((tp,))] * 2,
        compiler_params=pltpu.CompilerParams(
            collective_id=0, has_side_effects=True, vmem_limit_bytes=67043328
        ),
    )(
        *smalls,
        query_weight,
        key_weight,
        value_weight,
        key_cache,
        value_cache,
        out_weight,
    )
    return mixed, nk.reshape(seqs, kvc, width), nv.reshape(seqs, kvc, vd)


def choose(mesh_shape, *args):
    n, tp = mesh_shape
    seqs = args[0].shape[0]
    lh = args[8].shape[0]
    head_dim = args[2].shape[1] // (2 * lh)
    span = args[5].shape[2]
    vd = args[6].shape[3]
    fits = (
        n % 2 == 0
        and seqs % n == 0
        and (2 * (seqs // n) * lh) % 8 == 0
        and 2 * (seqs // n) * lh <= vd // 2
        and 2 * head_dim == vd == 128
        and span <= 256
        and (HEADS // KV_HEADS) % lh == 0
    )
    if fits:
        return fused_device(mesh_shape, *args)
    return per_device(*args)


def solution(mesh):
    return jax.shard_map(
        functools.partial(choose, (mesh.shape["kv"], mesh.shape["tp"])),
        mesh=mesh,
        in_specs=(
            P(),
            P(),
            P(None, "tp"),
            P(),
            P(),
            P(None, None, "kv", None),
            P(None, None, "kv", None),
            P(),
            P("tp"),
            P("tp", None),
            P("tp", "kv"),
        ),
        out_specs=(P(None, "kv"), P(), P()),
        check_vma=False,
    )
```

profile of v0, /device:TPU:0, one launch (start us, length us, event | category | flops | bytes accessed | tf_op | source)
XLA Modules:
  0.0 25.7 jit_solution(792092524205963288)
XLA Ops:
  0.6 21.0 %fused.1 = (bf16[32,192]{1,0:T(8,128)(2,1)}, bf16[32,256]{1,0:T(8,128)(2,1)}, bf16[32,256]{1,0:T(8,128)(2,1)}) custom-call(bf16[32,3072]{1,0:T(8,128)(2,1)} %hidden_h.1, bf16[3072]{0:T(1024)(128)(2,1)} %gain_h.1, s32[1,32]{1,0:T(1,128)} %bitcast.4, f32[1,6]{1,0:T(1,128)} %bitcast.5, bf16[6,128]{1,0:T(8,128)(2,1)} %head_gain_h.1, ...), custom_call_target="tpu_custom_call" | custom-call | tf_op jit(solution)/shard_map/fused/pallas_call | solution.py:557
  21.7 1.3 %reshape.20 = bf16[32,2,128]{2,1,0:T(2,128)(2,1)} reshape(bf16[32,256]{1,0:T(8,128)(2,1)} %get-tuple-element.7) | data formatting | bytes 32768 | tf_op jit(solution)/shard_map/reshape | solution.py:604
  23.0 1.3 %reshape.21 = bf16[32,2,128]{2,1,0:T(2,128)(2,1)} reshape(bf16[32,256]{1,0:T(8,128)(2,1)} %get-tuple-element.8) | data formatting | bytes 32768 | tf_op jit(solution)/shard_map/reshape | solution.py:604
  24.3 1.3 %copy.20 = bf16[32,192]{1,0:T(8,128)(2,1)} copy(bf16[32,192]{1,0:T(8,128)(2,1)} %get-tuple-element.12) | data formatting | bytes 24576
where the time goes:
time: 26.1 us; the launch traced here: 25.7 us
  Pallas kernels  21 us (80%)
  local copies, waits for them, and re-layouts  3.99 us (15%)
  between operations  0.64 us (2%)
    pallas_call x1, Pallas kernels, fused_device(): pl.pallas_call(functools.partial(fused_kernel, dims), name='fused', out_s...  21 us
    reshape x2, local copies, waits for them, and re-layouts, fused_device(): return (mixed, nk.reshape(seqs, kvc, width), nv.reshape(seqs, kvc, vd))  2.66 us
    unnamed x1, local copies, waits for them, and re-layouts  1.32 us

commit v1 on v0

--- a/solution.py
+++ b/solution.py
@@ -403,8 +403,8 @@
     for g in range(kvc):
         nk = turn(kp[:, g * width : (g + 1) * width]).astype(jnp.bfloat16)
         nv = vp[:, g * vd : (g + 1) * vd].astype(jnp.bfloat16)
-        new_keys[:, g * width : (g + 1) * width] = nk
-        new_values[:, g * vd : (g + 1) * vd] = nv
+        new_keys[:, g, :] = nk
+        new_values[:, g, :] = nv
         own_kv[0, g] = nk
         own_kv[1, g] = nv
     sr = lax.broadcasted_iota(jnp.int32, (ro, seqs), 0)
@@ -487,6 +487,16 @@
     for k in range(1, tp):
         summed = summed + pbuf[k].astype(jnp.float32)
     mixed[...] = summed.astype(jnp.bfloat16)
+
+
+def write_out(*refs):
+    copies = [
+        pltpu.make_async_copy(refs[i], refs[3 + i], refs[6].at[i]) for i in range(3)
+    ]
+    for cp in copies:
+        cp.start()
+    for cp in copies:
+        cp.wait()
 
 
 def tables(n, seqs, lh, span, head_dim, pad):
@@ -554,14 +564,11 @@
     )
     out_weight = jnp.transpose(out_weight)
     features = out_weight.shape[0]
-    mixed, nk, nv = pl.pallas_call(
+    results = ((seqs, features), (seqs, kvc, width), (seqs, kvc, vd))
+    held = pl.pallas_call(
         functools.partial(fused_kernel, dims),
         name="fused",
-        out_shape=(
-            jax.ShapeDtypeStruct((seqs, features), bf),
-            jax.ShapeDtypeStruct((seqs, kvc * width), bf),
-            jax.ShapeDtypeStruct((seqs, kvc * vd), bf),
-        ),
+        out_shape=tuple(pltpu.VMEM(shape, bf) for shape in results),
         in_specs=[hbm] * 16,
         out_specs=(vmem, vmem, vmem),
         scratch_shapes=[pltpu.VMEM(a.shape, a.dtype) for a in smalls]
@@ -590,18 +597,30 @@
         + [dma((n,))] * 4
         + [dma((tp,))] * 2,
         compiler_params=pltpu.CompilerParams(
-            collective_id=0, has_side_effects=True, vmem_limit_bytes=67043328
+            collective_id=0, has_side_effects=True, vmem_limit_bytes=32 * 1024 * 1024
         ),
     )(
-        *smalls,
-        query_weight,
-        key_weight,
-        value_weight,
-        key_cache,
-        value_cache,
-        out_weight,
-    )
-    return mixed, nk.reshape(seqs, kvc, width), nv.reshape(seqs, kvc, vd)
+        *(
+            pltpu.with_memory_space_constraint(a, pltpu.HBM)
+            for a in (
+                *smalls,
+                query_weight,
+                key_weight,
+                value_weight,
+                key_cache,
+                value_cache,
+                out_weight,
+            )
+        )
+    )
+    return pl.pallas_call(
+        write_out,
+        name="write_out",
+        out_shape=tuple(jax.ShapeDtypeStruct(shape, bf) for shape in results),
+        in_specs=[vmem] * 3,
+        out_specs=(hbm,) * 3,
+        scratch_shapes=[dma((3,))],
+    )(*(pltpu.with_memory_space_constraint(a, pltpu.VMEM) for a in held))
 
 
 def choose(mesh_shape, *args):

time: 26.1 us -> 21.8 us (0.84); the launches traced: 25.7 us -> 21.7 us
  local copies, waits for them, and re-layouts: 3.99 us -> 0 us
    reshape x2 -> x0, local copies, waits for them, and re-layouts: 2.66 us -> none  [fused_device(): return (mixed, nk.reshape(seqs, kvc, width), nv.reshape(seqs, kvc, vd))]
    unnamed x1 -> x0, local copies, waits for them, and re-layouts: 1.32 us -> none
    pallas_call x0 -> x1, Pallas kernels: none -> 0.65 us  [fused_device(): pl.pallas_call(write_out, name='write_out', out_shape=tuple((jax.ShapeDty...]
    pallas_call x1, Pallas kernels: 21 us -> 20.4 us  [fused_device(): pl.pallas_call(functools.partial(fused_kernel, dims), name='fused', out_s...]
where the time goes in v1:
time: 21.8 us; the launch traced here: 21.7 us
  Pallas kernels  21 us (96%)
  between operations  0.64 us (3%)
    pallas_call x1, Pallas kernels, fused_device(): pl.pallas_call(functools.partial(fused_kernel, dims), name='fused', out_s...  20.4 us
    pallas_call x1, Pallas kernels, fused_device(): pl.pallas_call(write_out, name='write_out', out_shape=tuple((jax.ShapeDty...  0.65 us

profile of v1, /device:TPU:0, one launch (start us, length us, event | category | flops | bytes accessed | tf_op | source)
XLA Modules:
  0.0 21.7 jit_solution(14391796694394236555)
XLA Ops:
  0.6 20.4 %fused.1 = (bf16[32,192]{1,0:T(8,128)(2,1)S(1)}, bf16[32,2,128]{2,1,0:T(2,128)(2,1)S(1)}, bf16[32,2,128]{2,1,0:T(2,128)(2,1)S(1)}) custom-call(bf16[32,3072]{1,0:T(8,128)(2,1)} %hidden_h.1, bf16[3072]{0:T(1024)(128)(2,1)} %gain_h.1, s32[1,32]{1,0:T(1,128)} %bitcast.4, f32[1,6]{1,0:T(1,128)} %bitcast.5, bf16[6,128]{1,0:T(8,128)(2,1)} %head_gain_h.1, ...), custom_call_target="tpu_custom_call" | custom-call | tf_op jit(solution)/shard_map/fused/pallas_call | solution.py:568
  21.0 0.6 %write_out.1 = (bf16[32,192]{1,0:T(8,128)(2,1)}, bf16[32,2,128]{2,1,0:T(2,128)(2,1)}, bf16[32,2,128]{2,1,0:T(2,128)(2,1)}) custom-call(bf16[32,192]{1,0:T(8,128)(2,1)S(1)} %get-tuple-element.6.refs_0_, bf16[32,2,128]{2,1,0:T(2,128)(2,1)S(1)} %get-tuple-element.7.refs_1_, bf16[32,2,128]{2,1,0:T(2,128)(2,1)S(1)} %get-tuple-element.8.refs_2_), custom_call_target="tpu_custom_call" | custom-call | tf_op jit(solution)/shard_map/write_out/pallas_call | solution.py:616
